TPU v7x, 32 devices: a whole 2x2x4 slice. The times are simulated.
32 devices in a mesh: fs: 8 (over z, core), tp: 4 (over y, x).
Axes of the slice: x: 2, y: 2, z: 4, core: 2. Of those that a mesh axis runs over, the one named last changes fastest.
Arguments:
- prompt: bfloat16 [1024, 2048], P('tp'), may hold values from -6 to 6
- norm_gain: float32 [2048], P('fs'), may hold values from 0.1 to 1.9
- gate_master: float32 [32, 2048, 512], P(None, 'fs', 'tp'), may hold values from -6 to 6
- up_master: float32 [32, 2048, 512], P(None, 'fs', 'tp'), may hold values from -6 to 6
- down_master: float32 [32, 2048, 512], P(None, 'fs', 'tp'), may hold values from -6 to 6
- group_choice: int32 [1024], P('tp'), may hold values from 0 to 3
- inner_choice: int32 [1024, 2], P('tp'), may hold values from 0 to 7, as said below
- route_weight: float32 [1024, 2], P('tp'), may hold values from 0.2 to 1
Outputs:
- gate_served: bfloat16 [2048, 16384], P(None, 'fs')
- up_served: bfloat16 [2048, 16384], P(None, 'fs')
- down_served: bfloat16 [2048, 16384], P(None, 'fs')
- mixed: bfloat16 [1024, 2048], P('tp', 'fs')
Inputs may be any that keep to these rules, and one draw needn't show every extreme that they name: `inner_choice`: the two experts of a token differ.
All inputs are finite; a program needn't handle non-finite values.
Results may differ from a plain program's by a relative error of at most 0.0081.
Values may be sent and summed in bfloat16 or wider, within the bound.
A program may use at most 128 MiB of HBM per device.

v0:
```python
import jax
import jax.numpy as jnp
from jax import lax
from jax.experimental import pallas as pl
from jax.experimental.pallas import tpu as pltpu
from jax.sharding import PartitionSpec as P

MESH = pl.DeviceIdType.MESH
FF = 512
GROUPS = 4
EPG = 8


def flatten_rows(piece):
    count, experts, rows, hidden = piece.shape
    return piece.transpose(0, 2, 1, 3).reshape(count, rows, experts * hidden)


def restore_rows(gathered, rows):
    parts = lax.axis_size("tp")
    count, total, width = gathered.shape
    blocks = total // (parts * rows)
    ordered = gathered.reshape(count, parts, blocks, rows, width).transpose(0, 2, 1, 3, 4)
    return ordered.reshape(count, total, width)


def activations(normed, gate_local, up_local, column_weight):
    width = normed.shape[1]
    gate_act = jnp.dot(normed, gate_local, preferred_element_type=jnp.float32) * width ** (-0.5)
    up_act = jnp.dot(normed, up_local, preferred_element_type=jnp.float32) * width ** (-0.5)
    return (column_weight * jax.nn.silu(gate_act) * up_act).astype(jnp.bfloat16)


def route_columns(weight, columns, experts):
    first = lax.axis_index("fs") * columns
    owner = (first + jnp.arange(columns, dtype=jnp.int32)) // FF
    onehot = (owner[None, :] == jnp.arange(experts, dtype=jnp.int32)[:, None]).astype(jnp.float32)
    return jnp.dot(weight, onehot, precision=lax.Precision.HIGHEST)


def shards(
    prompt, norm_gain, gate_master, up_master, down_master, group_choice, inner_choice, route_weight
):
    experts = GROUPS * EPG
    scale = norm_gain[None, :, None]
    gate_cast = (gate_master * scale).astype(jnp.bfloat16)
    up_cast = (up_master * scale).astype(jnp.bfloat16)
    down_cast = down_master.astype(jnp.bfloat16)
    rows = gate_master.shape[1] // lax.axis_size("tp")
    values = prompt.astype(jnp.float32)
    normed = (values * lax.rsqrt(jnp.mean(values * values, axis=1, keepdims=True) + 1e-06)).astype(
        jnp.bfloat16
    )
    chosen = group_choice[:, None] * EPG + inner_choice
    member = (chosen[:, :, None] == jnp.arange(experts, dtype=jnp.int32)[None, None, :]).astype(
        jnp.float32
    )
    weight = jnp.sum(member * route_weight[:, :, None], axis=1)
    stacked = jnp.stack([gate_cast, up_cast, down_cast])
    widened = lax.all_to_all(stacked, "tp", split_axis=2, concat_axis=3, tiled=True)
    moved = lax.all_to_all(flatten_rows(widened), "fs", split_axis=2, concat_axis=1, tiled=True)
    served = restore_rows(lax.all_gather(moved, "tp", axis=1, tiled=True), rows)
    gate_local, up_local, down_local = (served[0], served[1], served[2])
    column_weight = route_columns(weight, gate_local.shape[1], experts)
    scaled = activations(normed, gate_local, up_local, column_weight)
    summed = lax.psum_scatter(
        lax.dot_general(
            down_local, scaled, (((1,), (1,)), ((), ())), preferred_element_type=jnp.float32
        ),
        "fs",
        scatter_dimension=0,
        tiled=True,
    )
    mixed = (summed * FF ** (-0.5)).T.astype(jnp.bfloat16)
    return (gate_local, up_local, down_local, mixed)


def spread_body(
    gain_ref,
    gate_ref,
    up_ref,
    down_ref,
    prompt_ref,
    group_ref,
    inner_ref,
    route_ref,
    served,
    scaled,
    got,
    raw,
    cast,
    gain,
    scale,
    prompt,
    normed,
    group,
    inner,
    route,
    column,
    part,
    load_sem,
    small_sem,
    zs,
    zr,
    xs,
    xr,
    ys,
    yr,
    fxs,
    fxr,
    fys,
    fyr,
    ps,
    pr,
):
    f, t = lax.axis_index("fs"), lax.axis_index("tp")
    tx, ty, td = jnp.bitwise_xor(t, 1), jnp.bitwise_xor(t, 2), jnp.bitwise_xor(t, 3)
    arrays, groups, per, rows, hidden = raw.shape
    parts, tokens = served.shape[1], prompt.shape[0]
    half = rows // 2
    masters = (gate_ref, up_ref, down_ref)

    def peer(k):
        return jnp.bitwise_xor(f, k)

    def load(w, k):
        return pltpu.make_async_copy(masters[w].at[peer(k)], raw.at[w, k], load_sem.at[w, k])

    small = [
        pltpu.make_async_copy(source, target, small_sem.at[i])
        for i, (source, target) in enumerate(
            (
                (gain_ref, gain),
                (prompt_ref, prompt),
                (group_ref, group),
                (inner_ref, inner),
                (route_ref, route),
            )
        )
    ]

    def block(w, origin, k, begin=0, count=rows):
        first = pl.multiple_of(peer(k) * rows + begin, count)
        return served.at[w, origin, pl.ds(first, count)]

    def z_copy(w, k):
        return pltpu.make_async_remote_copy(
            src_ref=cast.at[w, k - 1],
            dst_ref=block(w, t, 0),
            send_sem=zs.at[w, k],
            recv_sem=zr.at[w, k],
            device_id={"fs": peer(k), "tp": t},
            device_id_type=MESH,
        )

    def z_arrival(w, k):
        return pltpu.make_async_remote_copy(
            src_ref=cast.at[w, k - 1],
            dst_ref=block(w, t, k),
            send_sem=zs.at[w, k],
            recv_sem=zr.at[w, k],
            device_id={"fs": peer(k), "tp": t},
            device_id_type=MESH,
        )

    def side_copy(w, k, origin, target, send, recv):
        return pltpu.make_async_remote_copy(
            src_ref=block(w, origin, k),
            dst_ref=block(w, origin, k),
            send_sem=send.at[w, k],
            recv_sem=recv.at[w, k],
            device_id={"fs": f, "tp": target},
            device_id_type=MESH,
        )

    def half_copy(w, k, origin, which, target, send, recv):
        piece = block(w, origin, k, which * half, half)
        return pltpu.make_async_remote_copy(
            src_ref=piece,
            dst_ref=piece,
            send_sem=send.at[w, k],
            recv_sem=recv.at[w, k],
            device_id={"fs": f, "tp": target},
            device_id_type=MESH,
        )

    def part_copy(k):
        return pltpu.make_async_remote_copy(
            src_ref=part.at[k - 1],
            dst_ref=got.at[k - 1],
            send_sem=ps.at[k],
            recv_sem=pr.at[k],
            device_id={"fs": peer(k), "tp": t},
            device_id_type=MESH,
        )

    def side_start(w, k):
        side_copy(w, k, t, tx, xs, xr).start()
        side_copy(w, k, t, ty, ys, yr).start()

    def forward(w, k):
        side_copy(w, k, tx, tx, xs, xr).wait_recv()
        half_copy(w, k, tx, 0, ty, fys, fyr).start()
        side_copy(w, k, ty, ty, ys, yr).wait_recv()
        half_copy(w, k, ty, 1, tx, fxs, fxr).start()

    def diagonal_wait(w, k):
        half_copy(w, k, td, 0, ty, fys, fyr).wait_recv()
        half_copy(w, k, td, 1, tx, fxs, fxr).wait_recv()

    def put(w, k, target):
        load(w, k).wait()
        for e in range(per):
            value = raw[w, k, e]
            if w < 2:
                value = value * scale[...]
            target[:, e * hidden : (e + 1) * hidden] = value.astype(jnp.bfloat16)

    def put_own(w):
        put(w, 0, block(w, t, 0))

    def put_away(w, k):
        put(w, k, cast.at[w, k - 1])

    def normalise():
        small[1].wait()
        values = prompt[...].astype(jnp.float32)
        mean = jnp.mean(values * values, axis=1, keepdims=True)
        normed[...] = (values * lax.rsqrt(mean + 1e-06)).astype(jnp.bfloat16)

    def columns():
        for i in range(2, 5):
            small[i].wait()
        chosen = group[...] * EPG + inner[...]
        for e in range(per):
            weight = jnp.sum(jnp.where(chosen == f * per + e, route[...], 0.0), axis=0, keepdims=True)
            column[:, e * hidden : (e + 1) * hidden] = jnp.broadcast_to(weight, (hidden, tokens)).T

    def hidden_units(origin):
        step = 2 * hidden
        for n in range(per // 2):
            at = pl.ds(n * step, step)
            scaled[origin, :, at] = activations(
                normed[...], served[0, origin, :, at], served[1, origin, :, at], column[:, at]
            )

    def features(k):
        total = None
        for i in range(parts):
            term = lax.dot_general(
                scaled[i],
                block(2, i, k)[...],
                (((1,), (1,)), ((), ())),
                preferred_element_type=jnp.float32,
            )
            total = term if total is None else total + term
        part[k - 1] = total.astype(jnp.bfloat16)

    last = list(range(groups - 1, -1, -1))
    order = [(w, k) for w in range(2) for k in range(groups)] + [(2, k) for k in last]
    away = [list(range(1, groups)), list(range(1, groups)), last[:-1]]

    small[0].start()
    load(0, 0).start()
    barrier = pltpu.get_barrier_semaphore()
    for k in range(1, groups):
        pl.semaphore_signal(barrier, inc=1, device_id={"fs": peer(k), "tp": t}, device_id_type=MESH)
    for other in (tx, ty):
        pl.semaphore_signal(barrier, inc=1, device_id={"fs": f, "tp": other}, device_id_type=MESH)
    for k in away[0]:
        load(0, k).start()
    for w in (1, 2):
        load(w, 0).start()
        for k in away[w]:
            load(w, k).start()
    for copy in small[1:]:
        copy.start()
    small[0].wait()
    scale[...] = jnp.broadcast_to(gain[...], (hidden, rows)).T
    put_own(0)
    put_away(0, 1)
    pl.semaphore_wait(barrier, groups + 1)
    side_start(0, 0)

    def first_away(k, carry):
        put_away(0, k)
        z_copy(0, k - 1).start()
        return carry

    lax.fori_loop(2, groups, first_away, 0)
    z_copy(0, groups - 1).start()

    def later_away(w):
        def one(k, carry):
            put_away(w, k)
            return carry

        put_own(w)
        lax.fori_loop(1, groups, one, 0)

    base = 2 * groups
    for s, (w, k) in enumerate(order):
        if s > 0:
            if k > 0:
                z_arrival(w, k).wait_recv()
            side_start(w, k)
            forward(*order[s - 1])
        if s == 0:
            later_away(1)
        if s == 1:
            later_away(2)
        if w < 2 and k > 0:
            z_copy(w + 1, away[w + 1][k - 1]).start()
        if s == groups:
            normalise()
            columns()
        if s == base:
            hidden_units(t)
        if s == base + 1:
            hidden_units(tx)
            hidden_units(ty)
        if s == base + 2:
            for i in range(base):
                diagonal_wait(*order[i])
            hidden_units(td)
        if s >= base + 2:
            one = order[s - 2][1]
            diagonal_wait(2, one)
            features(one)
            part_copy(one).start()
    forward(*order[-1])
    diagonal_wait(2, 1)
    features(1)
    part_copy(1).start()
    diagonal_wait(2, 0)

    def finish(w, carry):
        def one(k, inner):
            side_copy(w, k, t, tx, xs, xr).wait_send()
            side_copy(w, k, t, ty, ys, yr).wait_send()
            half_copy(w, k, tx, 0, ty, fys, fyr).wait_send()
            half_copy(w, k, ty, 1, tx, fxs, fxr).wait_send()
            return inner

        def two(k, inner):
            z_copy(w, k).wait_send()
            return inner

        lax.fori_loop(0, groups, one, 0)
        lax.fori_loop(1, groups, two, 0)
        return carry

    lax.fori_loop(0, arrays, finish, 0)
    for k in range(1, groups):
        part_copy(k).wait_recv()
        part_copy(k).wait_send()


def spread(prompt, norm_gain, gate_master, up_master, down_master, group_choice, inner_choice, route_weight):
    groups, parts = lax.axis_size("fs"), lax.axis_size("tp")
    experts, rows, hidden = gate_master.shape
    per = experts // groups
    tokens, width = prompt.shape
    arrays = 3
    views = [one.reshape(groups, per, rows, hidden) for one in (gate_master, up_master, down_master)]
    dma = pltpu.SemaphoreType.DMA
    return pl.pallas_call(
        spread_body,
        in_specs=[pl.BlockSpec(memory_space=pltpu.HBM)] * 8,
        out_specs=[pl.BlockSpec(memory_space=pltpu.VMEM)] * 3,
        out_shape=[
            pltpu.VMEM((arrays, parts, width, per * hidden), jnp.bfloat16),
            pltpu.VMEM((parts, tokens, per * hidden), jnp.bfloat16),
            pltpu.VMEM((groups - 1, tokens, rows), jnp.bfloat16),
        ],
        scratch_shapes=[
            pltpu.VMEM((arrays, groups, per, rows, hidden), jnp.float32),
            pltpu.VMEM((arrays, groups - 1, rows, per * hidden), jnp.bfloat16),
            pltpu.VMEM((1, rows), jnp.float32),
            pltpu.VMEM((rows, hidden), jnp.float32),
            pltpu.VMEM((tokens, width), jnp.bfloat16),
            pltpu.VMEM((tokens, width), jnp.bfloat16),
            pltpu.VMEM((1, tokens), jnp.int32),
            pltpu.VMEM((2, tokens), jnp.int32),
            pltpu.VMEM((2, tokens), jnp.float32),
            pltpu.VMEM((tokens, per * hidden), jnp.float32),
            pltpu.VMEM((groups - 1, tokens, rows), jnp.bfloat16),
            dma((arrays, groups)),
            dma((5,)),
        ]
        + [dma((arrays, groups))] * 10
        + [dma((groups,))] * 2,
        compiler_params=pltpu.CompilerParams(
            collective_id=0, has_side_effects=True, vmem_limit_bytes=32 * 1024 * 1024
        ),
        name="spread",
    )(
        norm_gain.reshape(1, rows),
        *views,
        prompt,
        group_choice.reshape(1, tokens),
        inner_choice.T,
        route_weight.T,
    )


def serve_body(served, scaled, got, gate_ref, up_ref, down_ref, mixed_ref, sem):
    arrays, parts, _, wide = served.shape
    rows = got.shape[2]
    hidden = FF // parts
    f = lax.axis_index("fs")
    copies = []
    for w, out in enumerate((gate_ref, up_ref, down_ref)):
        for i in range(parts):
            for e in range(wide // hidden):
                copies.append(
                    pltpu.make_async_copy(
                        served.at[w, i, :, pl.ds(e * hidden, hidden)],
                        out.at[:, pl.ds(e * FF + i * hidden, hidden)],
                        sem.at[len(copies)],
                    )
                )
    for copy in copies:
        copy.start()
    total = None
    for i in range(parts):
        term = lax.dot_general(
            scaled[i],
            served[2, i, pl.ds(pl.multiple_of(f * rows, rows), rows), :],
            (((1,), (1,)), ((), ())),
            preferred_element_type=jnp.float32,
        )
        total = term if total is None else total + term
    for k in range(got.shape[0]):
        total = total + got[k].astype(jnp.float32)
    mixed_ref[...] = (total * FF ** (-0.5)).astype(jnp.bfloat16)
    for copy in copies:
        copy.wait()


def serve(served, scaled, got):
    arrays, parts, width, wide = served.shape
    _, tokens, rows = got.shape
    out = jax.ShapeDtypeStruct((width, parts * wide), served.dtype)
    vmem, hbm = pl.BlockSpec(memory_space=pltpu.VMEM), pl.BlockSpec(memory_space=pltpu.HBM)
    return pl.pallas_call(
        serve_body,
        in_specs=[vmem, vmem, vmem],
        out_specs=[hbm, hbm, hbm, vmem],
        out_shape=[out, out, out, jax.ShapeDtypeStruct((tokens, rows), jnp.bfloat16)],
        scratch_shapes=[pltpu.SemaphoreType.DMA((arrays * parts * (parts * wide // FF),))],
        compiler_params=pltpu.CompilerParams(vmem_limit_bytes=4 * 1024 * 1024),
        name="serve",
    )(*[pltpu.with_memory_space_constraint(one, pltpu.VMEM) for one in (served, scaled, got)])


def direct_shards(
    prompt, norm_gain, gate_master, up_master, down_master, group_choice, inner_choice, route_weight
):
    served, scaled, got = spread(
        prompt, norm_gain, gate_master, up_master, down_master, group_choice, inner_choice, route_weight
    )
    return tuple(serve(served, scaled, got))


def fits_direct(mesh):
    groups, parts = mesh.shape["fs"], mesh.shape["tp"]
    whole_experts = (GROUPS * EPG) % groups == 0 and (GROUPS * EPG // groups) % 2 == 0
    return parts == 4 and groups >= 4 and groups & (groups - 1) == 0 and whole_experts and FF // parts % 128 == 0


def solution(mesh):
    in_specs = (
        P("tp", None),
        P("fs"),
        P(None, "fs", "tp"),
        P(None, "fs", "tp"),
        P(None, "fs", "tp"),
        P("tp"),
        P("tp", None),
        P("tp", None),
    )
    out_specs = (P(None, "fs"), P(None, "fs"), P(None, "fs"), P("tp", "fs"))
    body = direct_shards if fits_direct(mesh) else shards
    return jax.shard_map(body, mesh=mesh, in_specs=in_specs, out_specs=out_specs, check_vma=False)
```

profile of v0, /device:TPU:1, one launch (start us, length us, event | category | flops | bytes accessed | tf_op | source)
XLA Modules:
  0.0 226.7 jit_solution(5739287309214259404)
XLA Ops:
  0.6 216.3 %spread.1 = (bf16[3,4,2048,512]{3,2,1,0:T(8,128)(2,1)S(1)}, bf16[4,256,512]{2,1,0:T(8,128)(2,1)S(1)}, bf16[7,256,256]{2,1,0:T(8,128)(2,1)S(1)}) custom-call(f32[1,256]{1,0:T(1,128)} %bitcast.12, f32[8,4,256,128]{3,2,1,0:T(8,128)} %bitcast.7, f32[8,4,256,128]{3,2,1,0:T(8,128)} %bitcast.8, f32[8,4,256,128]{3,2,1,0:T(8,128)} %bitcast.9, ...), custom_call_target="tpu_custom_call" | custom-call | tf_op jit(solution)/shard_map/spread/pallas_call | solution.py:367
  217.0 9.7 %serve.1 = (bf16[2048,2048]{1,0:T(8,128)(2,1)}, bf16[2048,2048]{1,0:T(8,128)(2,1)}, bf16[2048,2048]{1,0:T(8,128)(2,1)}, bf16[256,256]{1,0:T(8,128)(2,1)}) custom-call(bf16[3,4,2048,512]{3,2,1,0:T(8,128)(2,1)S(1)} %get-tuple-element.7.served, bf16[4,256,512]{2,1,0:T(8,128)(2,1)S(1)} %get-tuple-element.8.scaled, bf16[7,256,256]{2,1,0:T(8,128)(2,1)S(1)} %get-tuple-element.9.got), custom_call_target="tpu_custom_call" | custom-call | tf_op jit(solution)/shard_map/serve/pallas_call | solution.py:446
where the time goes:
time: 228 us; the launch traced here: 227 us
  Pallas kernels  226 us (99%)
    pallas_call x1, Pallas kernels, spread(): pl.pallas_call(spread_body, in_specs=[pl.BlockSpec(memory_space=pltpu.HBM...  216 us
    pallas_call x1, Pallas kernels, serve(): pl.pallas_call(serve_body, in_specs=[vmem, vmem, vmem], out_specs=[hbm, h...  9.69 us

commit v1 on v0

--- a/solution.py
+++ b/solution.py
@@ -99,32 +99,44 @@
     column,
     part,
     load_sem,
+    bulk_sem,
     small_sem,
-    zs,
+    send_sem,
     zr,
-    xs,
     xr,
-    ys,
     yr,
-    fxs,
-    fxr,
-    fys,
-    fyr,
-    ps,
+    dr,
     pr,
 ):
     f, t = lax.axis_index("fs"), lax.axis_index("tp")
     tx, ty, td = jnp.bitwise_xor(t, 1), jnp.bitwise_xor(t, 2), jnp.bitwise_xor(t, 3)
     arrays, groups, per, rows, hidden = raw.shape
-    parts, tokens = served.shape[1], prompt.shape[0]
+    parts, width = served.shape[1:3]
+    tokens = prompt.shape[0]
     half = rows // 2
     masters = (gate_ref, up_ref, down_ref)
+    near = [2 * (i ^ (i >> 1)) + c for i in range(groups // 2) for c in range(2)]
+    last = near[::-1]
+    order = [(w, k) for w in range(2) for k in near] + [(2, k) for k in last]
 
     def peer(k):
         return jnp.bitwise_xor(f, k)
 
-    def load(w, k):
-        return pltpu.make_async_copy(masters[w].at[peer(k)], raw.at[w, k], load_sem.at[w, k])
+    def remote(source, target, send, recv, device):
+        return pltpu.make_async_remote_copy(
+            src_ref=source,
+            dst_ref=target,
+            send_sem=send,
+            recv_sem=recv,
+            device_id=device,
+            device_id_type=MESH,
+        )
+
+    def load(k):
+        return pltpu.make_async_copy(gate_ref.at[peer(k)], raw.at[0, peer(k)], load_sem.at[k])
+
+    def bulk(w):
+        return pltpu.make_async_copy(masters[w], raw.at[w], bulk_sem.at[w - 1])
 
     small = [
         pltpu.make_async_copy(source, target, small_sem.at[i])
@@ -144,83 +156,63 @@
         return served.at[w, origin, pl.ds(first, count)]
 
     def z_copy(w, k):
-        return pltpu.make_async_remote_copy(
-            src_ref=cast.at[w, k - 1],
-            dst_ref=block(w, t, 0),
-            send_sem=zs.at[w, k],
-            recv_sem=zr.at[w, k],
-            device_id={"fs": peer(k), "tp": t},
-            device_id_type=MESH,
-        )
+        device = {"fs": peer(k), "tp": t}
+        return remote(cast.at[w, k - 1], block(w, t, 0), send_sem.at[2], zr.at[w, k - 1], device)
 
     def z_arrival(w, k):
-        return pltpu.make_async_remote_copy(
-            src_ref=cast.at[w, k - 1],
-            dst_ref=block(w, t, k),
-            send_sem=zs.at[w, k],
-            recv_sem=zr.at[w, k],
-            device_id={"fs": peer(k), "tp": t},
-            device_id_type=MESH,
-        )
-
-    def side_copy(w, k, origin, target, send, recv):
-        return pltpu.make_async_remote_copy(
-            src_ref=block(w, origin, k),
-            dst_ref=block(w, origin, k),
-            send_sem=send.at[w, k],
-            recv_sem=recv.at[w, k],
-            device_id={"fs": f, "tp": target},
-            device_id_type=MESH,
-        )
-
-    def half_copy(w, k, origin, which, target, send, recv):
-        piece = block(w, origin, k, which * half, half)
-        return pltpu.make_async_remote_copy(
-            src_ref=piece,
-            dst_ref=piece,
-            send_sem=send.at[w, k],
-            recv_sem=recv.at[w, k],
-            device_id={"fs": f, "tp": target},
-            device_id_type=MESH,
-        )
+        device = {"fs": peer(k), "tp": t}
+        return remote(cast.at[w, k - 1], block(w, t, k), send_sem.at[2], zr.at[w, k - 1], device)
+
+    def x_copy(s, origin):
+        one = block(order[s][0], origin, order[s][1])
+        return remote(one, one, send_sem.at[0], xr.at[s % groups], {"fs": f, "tp": tx})
+
+    def y_copy(s, origin):
+        one = block(order[s][0], origin, order[s][1])
+        return remote(one, one, send_sem.at[1], yr.at[s % groups], {"fs": f, "tp": ty})
+
+    def to_x(s):
+        one = block(order[s][0], ty, order[s][1], half, half)
+        return remote(one, one, send_sem.at[0], dr.at[s % groups], {"fs": f, "tp": tx})
+
+    def to_y(s):
+        one = block(order[s][0], tx, order[s][1], 0, half)
+        return remote(one, one, send_sem.at[1], dr.at[s % groups], {"fs": f, "tp": ty})
+
+    def diagonal_wait(s):
+        one = block(order[s][0], td, order[s][1])
+        remote(one, one, send_sem.at[0], dr.at[s % groups], {"fs": f, "tp": tx}).wait_recv()
 
     def part_copy(k):
-        return pltpu.make_async_remote_copy(
-            src_ref=part.at[k - 1],
-            dst_ref=got.at[k - 1],
-            send_sem=ps.at[k],
-            recv_sem=pr.at[k],
-            device_id={"fs": peer(k), "tp": t},
-            device_id_type=MESH,
-        )
-
-    def side_start(w, k):
-        side_copy(w, k, t, tx, xs, xr).start()
-        side_copy(w, k, t, ty, ys, yr).start()
-
-    def forward(w, k):
-        side_copy(w, k, tx, tx, xs, xr).wait_recv()
-        half_copy(w, k, tx, 0, ty, fys, fyr).start()
-        side_copy(w, k, ty, ty, ys, yr).wait_recv()
-        half_copy(w, k, ty, 1, tx, fxs, fxr).start()
-
-    def diagonal_wait(w, k):
-        half_copy(w, k, td, 0, ty, fys, fyr).wait_recv()
-        half_copy(w, k, td, 1, tx, fxs, fxr).wait_recv()
+        device = {"fs": peer(k), "tp": t}
+        return remote(part.at[k - 1], got.at[k - 1], send_sem.at[3], pr, device)
+
+    def side_start(s):
+        x_copy(s, t).start()
+        y_copy(s, t).start()
+
+    def forward(s):
+        x_copy(s, tx).wait_recv()
+        to_y(s).start()
+        y_copy(s, ty).wait_recv()
+        to_x(s).start()
 
     def put(w, k, target):
-        load(w, k).wait()
         for e in range(per):
-            value = raw[w, k, e]
+            value = raw[w, peer(k), e]
             if w < 2:
                 value = value * scale[...]
             target[:, e * hidden : (e + 1) * hidden] = value.astype(jnp.bfloat16)
 
-    def put_own(w):
+    def put_all(w):
+        bulk(w).wait()
         put(w, 0, block(w, t, 0))
 
-    def put_away(w, k):
-        put(w, k, cast.at[w, k - 1])
+        def one(k, carry):
+            put(w, k, cast.at[w, k - 1])
+            return carry
+
+        lax.fori_loop(1, groups, one, 0)
 
     def normalise():
         small[1].wait()
@@ -256,104 +248,74 @@
             total = term if total is None else total + term
         part[k - 1] = total.astype(jnp.bfloat16)
 
-    last = list(range(groups - 1, -1, -1))
-    order = [(w, k) for w in range(2) for k in range(groups)] + [(2, k) for k in last]
-    away = [list(range(1, groups)), list(range(1, groups)), last[:-1]]
-
     small[0].start()
-    load(0, 0).start()
+    load(0).start()
     barrier = pltpu.get_barrier_semaphore()
     for k in range(1, groups):
         pl.semaphore_signal(barrier, inc=1, device_id={"fs": peer(k), "tp": t}, device_id_type=MESH)
     for other in (tx, ty):
         pl.semaphore_signal(barrier, inc=1, device_id={"fs": f, "tp": other}, device_id_type=MESH)
-    for k in away[0]:
-        load(0, k).start()
+    for k in near[1:]:
+        load(k).start()
     for w in (1, 2):
-        load(w, 0).start()
-        for k in away[w]:
-            load(w, k).start()
+        bulk(w).start()
     for copy in small[1:]:
         copy.start()
     small[0].wait()
     scale[...] = jnp.broadcast_to(gain[...], (hidden, rows)).T
-    put_own(0)
-    put_away(0, 1)
+    load(0).wait()
+    put(0, 0, block(0, t, 0))
+    load(near[1]).wait()
+    put(0, near[1], cast.at[0, near[1] - 1])
     pl.semaphore_wait(barrier, groups + 1)
-    side_start(0, 0)
-
-    def first_away(k, carry):
-        put_away(0, k)
-        z_copy(0, k - 1).start()
-        return carry
-
-    lax.fori_loop(2, groups, first_away, 0)
-    z_copy(0, groups - 1).start()
-
-    def later_away(w):
-        def one(k, carry):
-            put_away(w, k)
-            return carry
-
-        put_own(w)
-        lax.fori_loop(1, groups, one, 0)
-
-    base = 2 * groups
+    side_start(0)
+    for before, k in zip(near[1:], near[2:]):
+        load(k).wait()
+        put(0, k, cast.at[0, k - 1])
+        z_copy(0, before).start()
+    z_copy(0, last[0]).start()
+
+    base, lag = 2 * groups, groups // 2
+    sends = [(lag if i < 3 else lag + (i + 1) // 2, 1, k) for i, k in enumerate(near[1:])]
+    sends += [(groups + 3 + i // 2, 2, k) for i, k in enumerate(last[:-1])]
     for s, (w, k) in enumerate(order):
         if s > 0:
             if k > 0:
                 z_arrival(w, k).wait_recv()
-            side_start(w, k)
-            forward(*order[s - 1])
-        if s == 0:
-            later_away(1)
-        if s == 1:
-            later_away(2)
-        if w < 2 and k > 0:
-            z_copy(w + 1, away[w + 1][k - 1]).start()
+            side_start(s)
+            forward(s - 1)
+        for at, array, one in sends:
+            if at == s:
+                z_copy(array, one).start()
+        if s < 2:
+            put_all(s + 1)
         if s == groups:
             normalise()
             columns()
+        if 3 <= s < base + 2:
+            diagonal_wait(s - 3)
         if s == base:
             hidden_units(t)
         if s == base + 1:
             hidden_units(tx)
             hidden_units(ty)
         if s == base + 2:
-            for i in range(base):
-                diagonal_wait(*order[i])
+            diagonal_wait(base - 1)
             hidden_units(td)
         if s >= base + 2:
-            one = order[s - 2][1]
-            diagonal_wait(2, one)
-            features(one)
-            part_copy(one).start()
-    forward(*order[-1])
-    diagonal_wait(2, 1)
+            diagonal_wait(s - 2)
+            features(order[s - 2][1])
+            part_copy(order[s - 2][1]).start()
+    count = len(order)
+    forward(count - 1)
+    diagonal_wait(count - 2)
     features(1)
     part_copy(1).start()
-    diagonal_wait(2, 0)
-
-    def finish(w, carry):
-        def one(k, inner):
-            side_copy(w, k, t, tx, xs, xr).wait_send()
-            side_copy(w, k, t, ty, ys, yr).wait_send()
-            half_copy(w, k, tx, 0, ty, fys, fyr).wait_send()
-            half_copy(w, k, ty, 1, tx, fxs, fxr).wait_send()
-            return inner
-
-        def two(k, inner):
-            z_copy(w, k).wait_send()
-            return inner
-
-        lax.fori_loop(0, groups, one, 0)
-        lax.fori_loop(1, groups, two, 0)
-        return carry
-
-    lax.fori_loop(0, arrays, finish, 0)
-    for k in range(1, groups):
-        part_copy(k).wait_recv()
-        part_copy(k).wait_send()
+    diagonal_wait(count - 1)
+    sent = served.at[:, pl.ds(0, parts - 1), pl.ds(0, width // 2)]
+    for i, whole in enumerate((sent, sent, cast, part)):
+        remote(whole, whole, send_sem.at[i], pr, {"fs": f, "tp": tx}).wait_send()
+    remote(got, got, send_sem.at[3], pr, {"fs": f, "tp": tx}).wait_recv()
 
 
 def spread(prompt, norm_gain, gate_master, up_master, down_master, group_choice, inner_choice, route_weight):
@@ -385,11 +347,16 @@
             pltpu.VMEM((2, tokens), jnp.float32),
             pltpu.VMEM((tokens, per * hidden), jnp.float32),
             pltpu.VMEM((groups - 1, tokens, rows), jnp.bfloat16),
-            dma((arrays, groups)),
+            dma((groups,)),
+            dma((2,)),
             dma((5,)),
-        ]
-        + [dma((arrays, groups))] * 10
-        + [dma((groups,))] * 2,
+            dma((4,)),
+            dma((arrays, groups - 1)),
+            dma((groups,)),
+            dma((groups,)),
+            dma((groups,)),
+            dma,
+        ],
         compiler_params=pltpu.CompilerParams(
             collective_id=0, has_side_effects=True, vmem_limit_bytes=32 * 1024 * 1024
         ),
@@ -404,24 +371,20 @@
     )
 
 
-def serve_body(served, scaled, got, gate_ref, up_ref, down_ref, mixed_ref, sem):
+def serve_body(served, scaled, got, gate_ref, up_ref, down_ref, mixed_ref, mixed, sem):
     arrays, parts, _, wide = served.shape
     rows = got.shape[2]
     hidden = FF // parts
     f = lax.axis_index("fs")
-    copies = []
-    for w, out in enumerate((gate_ref, up_ref, down_ref)):
+    outs = (gate_ref, up_ref, down_ref)
+    for w, out in enumerate(outs):
         for i in range(parts):
             for e in range(wide // hidden):
-                copies.append(
-                    pltpu.make_async_copy(
-                        served.at[w, i, :, pl.ds(e * hidden, hidden)],
-                        out.at[:, pl.ds(e * FF + i * hidden, hidden)],
-                        sem.at[len(copies)],
-                    )
-                )
-    for copy in copies:
-        copy.start()
+                pltpu.make_async_copy(
+                    served.at[w, i, :, pl.ds(e * hidden, hidden)],
+                    out.at[:, pl.ds(e * FF + i * hidden, hidden)],
+                    sem.at[w],
+                ).start()
     total = None
     for i in range(parts):
         term = lax.dot_general(
@@ -433,9 +396,12 @@
         total = term if total is None else total + term
     for k in range(got.shape[0]):
         total = total + got[k].astype(jnp.float32)
-    mixed_ref[...] = (total * FF ** (-0.5)).astype(jnp.bfloat16)
-    for copy in copies:
-        copy.wait()
+    mixed[...] = (total * FF ** (-0.5)).astype(jnp.bfloat16)
+    final = pltpu.make_async_copy(mixed, mixed_ref, sem.at[arrays])
+    final.start()
+    for w, out in enumerate(outs):
+        pltpu.make_async_copy(out, out, sem.at[w]).wait()
+    final.wait()
 
 
 def serve(served, scaled, got):
@@ -446,9 +412,9 @@
     return pl.pallas_call(
         serve_body,
         in_specs=[vmem, vmem, vmem],
-        out_specs=[hbm, hbm, hbm, vmem],
+        out_specs=[hbm, hbm, hbm, hbm],
         out_shape=[out, out, out, jax.ShapeDtypeStruct((tokens, rows), jnp.bfloat16)],
-        scratch_shapes=[pltpu.SemaphoreType.DMA((arrays * parts * (parts * wide // FF),))],
+        scratch_shapes=[pltpu.VMEM((tokens, rows), jnp.bfloat16), pltpu.SemaphoreType.DMA((arrays + 1,))],
         compiler_params=pltpu.CompilerParams(vmem_limit_bytes=4 * 1024 * 1024),
         name="serve",
     )(*[pltpu.with_memory_space_constraint(one, pltpu.VMEM) for one in (served, scaled, got)])

time: 228 us -> 220 us (0.965)
  Pallas kernels: 226 us -> 218 us
    pallas_call x1, Pallas kernels: 216 us -> 210 us  [spread(): pl.pallas_call(spread_body, in_specs=[pl.BlockSpec(memory_space=pltpu.HBM...]
where the time goes in v1:
time: 220 us; the launch traced here: 219 us
  Pallas kernels  218 us (99%)
    pallas_call x1, Pallas kernels, spread(): pl.pallas_call(spread_body, in_specs=[pl.BlockSpec(memory_space=pltpu.HBM...  210 us
    pallas_call x1, Pallas kernels, serve(): pl.pallas_call(serve_body, in_specs=[vmem, vmem, vmem], out_specs=[hbm, h...  8.66 us

profile of v1, /device:TPU:1, one launch (start us, length us, event | category | flops | bytes accessed | tf_op | source)
XLA Modules:
  0.0 219.1 jit_solution(11466603445614618258)
XLA Ops:
  0.6 209.8 %spread.1 = (bf16[3,4,2048,512]{3,2,1,0:T(8,128)(2,1)S(1)}, bf16[4,256,512]{2,1,0:T(8,128)(2,1)S(1)}, bf16[7,256,256]{2,1,0:T(8,128)(2,1)S(1)}) custom-call(f32[1,256]{1,0:T(1,128)} %bitcast.12, f32[8,4,256,128]{3,2,1,0:T(8,128)} %bitcast.7, f32[8,4,256,128]{3,2,1,0:T(8,128)} %bitcast.8, f32[8,4,256,128]{3,2,1,0:T(8,128)} %bitcast.9, ...), custom_call_target="tpu_custom_call" | custom-call | tf_op jit(solution)/shard_map/spread/pallas_call | solution.py:329
  210.4 8.7 %serve.1 = (bf16[2048,2048]{1,0:T(8,128)(2,1)}, bf16[2048,2048]{1,0:T(8,128)(2,1)}, bf16[2048,2048]{1,0:T(8,128)(2,1)}, bf16[256,256]{1,0:T(8,128)(2,1)}) custom-call(bf16[3,4,2048,512]{3,2,1,0:T(8,128)(2,1)S(1)} %get-tuple-element.7.served, bf16[4,256,512]{2,1,0:T(8,128)(2,1)S(1)} %get-tuple-element.8.scaled, bf16[7,256,256]{2,1,0:T(8,128)(2,1)S(1)} %get-tuple-element.9.got), custom_call_target="tpu_custom_call" | custom-call | tf_op jit(solution)/shard_map/serve/pallas_call | solution.py:412

commit v2 on v1

--- a/solution.py
+++ b/solution.py
@@ -75,6 +75,27 @@
     return (gate_local, up_local, down_local, mixed)
 
 
+def remote(source, target, send, recv, device):
+    return pltpu.make_async_remote_copy(
+        src_ref=source,
+        dst_ref=target,
+        send_sem=send,
+        recv_sem=recv,
+        device_id=device,
+        device_id_type=MESH,
+    )
+
+
+def block_order(groups):
+    near = [2 * (i ^ (i >> 1)) + c for i in range(groups // 2) for c in range(2)]
+    last = near[::-1]
+    return near, [k for k in last if k % 2 == 1], [k for k in last if k % 2 == 0]
+
+
+def matmul_nt(left, right):
+    return lax.dot_general(left, right, (((1,), (1,)), ((), ())), preferred_element_type=jnp.float32)
+
+
 def spread_body(
     gain_ref,
     gate_ref,
@@ -84,7 +105,8 @@
     group_ref,
     inner_ref,
     route_ref,
-    served,
+    wide,
+    down,
     scaled,
     got,
     raw,
@@ -111,26 +133,16 @@
     f, t = lax.axis_index("fs"), lax.axis_index("tp")
     tx, ty, td = jnp.bitwise_xor(t, 1), jnp.bitwise_xor(t, 2), jnp.bitwise_xor(t, 3)
     arrays, groups, per, rows, hidden = raw.shape
-    parts, width = served.shape[1:3]
+    parts, width = down.shape[:2]
     tokens = prompt.shape[0]
     half = rows // 2
     masters = (gate_ref, up_ref, down_ref)
-    near = [2 * (i ^ (i >> 1)) + c for i in range(groups // 2) for c in range(2)]
-    last = near[::-1]
-    order = [(w, k) for w in range(2) for k in near] + [(2, k) for k in last]
+    near, odds, evens = block_order(groups)
+    order = [(w, k) for w in range(2) for k in near] + [(2, k) for k in odds + evens]
+    base, split, lag = 2 * groups, 2 * groups + len(odds), groups // 2
 
     def peer(k):
         return jnp.bitwise_xor(f, k)
-
-    def remote(source, target, send, recv, device):
-        return pltpu.make_async_remote_copy(
-            src_ref=source,
-            dst_ref=target,
-            send_sem=send,
-            recv_sem=recv,
-            device_id=device,
-            device_id_type=MESH,
-        )
 
     def load(k):
         return pltpu.make_async_copy(gate_ref.at[peer(k)], raw.at[0, peer(k)], load_sem.at[k])
@@ -152,40 +164,36 @@
     ]
 
     def block(w, origin, k, begin=0, count=rows):
-        first = pl.multiple_of(peer(k) * rows + begin, count)
-        return served.at[w, origin, pl.ds(first, count)]
+        at = pl.ds(pl.multiple_of(peer(k) * rows + begin, count), count)
+        return wide.at[w, origin, at] if w < 2 else down.at[origin, at]
 
     def z_copy(w, k):
         device = {"fs": peer(k), "tp": t}
-        return remote(cast.at[w, k - 1], block(w, t, 0), send_sem.at[2], zr.at[w, k - 1], device)
+        return remote(cast.at[w, k - 1], block(w, t, 0), send_sem.at[4], zr.at[w, k - 1], device)
 
     def z_arrival(w, k):
         device = {"fs": peer(k), "tp": t}
-        return remote(cast.at[w, k - 1], block(w, t, k), send_sem.at[2], zr.at[w, k - 1], device)
+        return remote(cast.at[w, k - 1], block(w, t, k), send_sem.at[4], zr.at[w, k - 1], device)
 
     def x_copy(s, origin):
         one = block(order[s][0], origin, order[s][1])
-        return remote(one, one, send_sem.at[0], xr.at[s % groups], {"fs": f, "tp": tx})
+        return remote(one, one, send_sem.at[s // base], xr.at[s % groups], {"fs": f, "tp": tx})
 
     def y_copy(s, origin):
         one = block(order[s][0], origin, order[s][1])
-        return remote(one, one, send_sem.at[1], yr.at[s % groups], {"fs": f, "tp": ty})
+        return remote(one, one, send_sem.at[2 + s // base], yr.at[s % groups], {"fs": f, "tp": ty})
 
     def to_x(s):
         one = block(order[s][0], ty, order[s][1], half, half)
-        return remote(one, one, send_sem.at[0], dr.at[s % groups], {"fs": f, "tp": tx})
+        return remote(one, one, send_sem.at[s // base], dr.at[s % groups], {"fs": f, "tp": tx})
 
     def to_y(s):
         one = block(order[s][0], tx, order[s][1], 0, half)
-        return remote(one, one, send_sem.at[1], dr.at[s % groups], {"fs": f, "tp": ty})
+        return remote(one, one, send_sem.at[2 + s // base], dr.at[s % groups], {"fs": f, "tp": ty})
 
     def diagonal_wait(s):
         one = block(order[s][0], td, order[s][1])
         remote(one, one, send_sem.at[0], dr.at[s % groups], {"fs": f, "tp": tx}).wait_recv()
-
-    def part_copy(k):
-        device = {"fs": peer(k), "tp": t}
-        return remote(part.at[k - 1], got.at[k - 1], send_sem.at[3], pr, device)
 
     def side_start(s):
         x_copy(s, t).start()
@@ -233,20 +241,18 @@
         for n in range(per // 2):
             at = pl.ds(n * step, step)
             scaled[origin, :, at] = activations(
-                normed[...], served[0, origin, :, at], served[1, origin, :, at], column[:, at]
+                normed[...], wide[0, origin, :, at], wide[1, origin, :, at], column[:, at]
             )
 
-    def features(k):
-        total = None
-        for i in range(parts):
-            term = lax.dot_general(
-                scaled[i],
-                block(2, i, k)[...],
-                (((1,), (1,)), ((), ())),
-                preferred_element_type=jnp.float32,
-            )
-            total = term if total is None else total + term
-        part[k - 1] = total.astype(jnp.bfloat16)
+    def features(s):
+        k = order[s][1]
+        diagonal_wait(s)
+        total = matmul_nt(scaled[0], block(2, 0, k)[...])
+        for i in range(1, parts):
+            total = total + matmul_nt(scaled[i], block(2, i, k)[...])
+        part[s - base] = total.astype(jnp.bfloat16)
+        device = {"fs": peer(k), "tp": t}
+        remote(part.at[s - base], got.at[k - 1], send_sem.at[5], pr, device).start()
 
     small[0].start()
     load(0).start()
@@ -273,12 +279,13 @@
         load(k).wait()
         put(0, k, cast.at[0, k - 1])
         z_copy(0, before).start()
-    z_copy(0, last[0]).start()
-
-    base, lag = 2 * groups, groups // 2
+    z_copy(0, near[-1]).start()
+
     sends = [(lag if i < 3 else lag + (i + 1) // 2, 1, k) for i, k in enumerate(near[1:])]
-    sends += [(groups + 3 + i // 2, 2, k) for i, k in enumerate(last[:-1])]
-    for s, (w, k) in enumerate(order):
+    sends += [(groups + 3 + i // 2, 2, k) for i, k in enumerate(near[:0:-1])]
+
+    def step(s):
+        w, k = order[s]
         if s > 0:
             if k > 0:
                 z_arrival(w, k).wait_recv()
@@ -303,19 +310,38 @@
             diagonal_wait(base - 1)
             hidden_units(td)
         if s >= base + 2:
-            diagonal_wait(s - 2)
-            features(order[s - 2][1])
-            part_copy(order[s - 2][1]).start()
-    count = len(order)
-    forward(count - 1)
-    diagonal_wait(count - 2)
-    features(1)
-    part_copy(1).start()
-    diagonal_wait(count - 1)
-    sent = served.at[:, pl.ds(0, parts - 1), pl.ds(0, width // 2)]
-    for i, whole in enumerate((sent, sent, cast, part)):
-        remote(whole, whole, send_sem.at[i], pr, {"fs": f, "tp": tx}).wait_send()
-    remote(got, got, send_sem.at[3], pr, {"fs": f, "tp": tx}).wait_recv()
+            features(s - 2)
+
+    def drain(end):
+        forward(end - 1)
+        features(end - 2)
+        if order[end - 1][1] > 0:
+            features(end - 1)
+        else:
+            diagonal_wait(end - 1)
+        count = end - base
+        sums = min(count, groups - 1)
+        first = wide.at[:, pl.ds(0, parts - 1), pl.ds(0, width // 2)]
+        second = down.at[pl.ds(0, parts - 1), pl.ds(0, count * half)]
+        for i, whole in enumerate((first, second, first, second, cast, part.at[pl.ds(0, sums)])):
+            remote(whole, whole, send_sem.at[i], pr, {"fs": f, "tp": tx}).wait_send()
+        whole = got.at[pl.ds(0, sums)]
+        remote(whole, whole, send_sem.at[5], pr, {"fs": f, "tp": tx}).wait_recv()
+
+    for s in range(split):
+        step(s)
+
+    @pl.when(f % 2 == 0)
+    def _():
+        for k in evens[:-1]:
+            z_arrival(2, k).wait_recv()
+        drain(split)
+
+    @pl.when(f % 2 == 1)
+    def _():
+        for s in range(split, len(order)):
+            step(s)
+        drain(len(order))
 
 
 def spread(prompt, norm_gain, gate_master, up_master, down_master, group_choice, inner_choice, route_weight):
@@ -329,9 +355,10 @@
     return pl.pallas_call(
         spread_body,
         in_specs=[pl.BlockSpec(memory_space=pltpu.HBM)] * 8,
-        out_specs=[pl.BlockSpec(memory_space=pltpu.VMEM)] * 3,
+        out_specs=[pl.BlockSpec(memory_space=pltpu.VMEM)] * 4,
         out_shape=[
-            pltpu.VMEM((arrays, parts, width, per * hidden), jnp.bfloat16),
+            pltpu.VMEM((2, parts, width, per * hidden), jnp.bfloat16),
+            pltpu.VMEM((parts, width, per * hidden), jnp.bfloat16),
             pltpu.VMEM((parts, tokens, per * hidden), jnp.bfloat16),
             pltpu.VMEM((groups - 1, tokens, rows), jnp.bfloat16),
         ],
@@ -350,7 +377,7 @@
             dma((groups,)),
             dma((2,)),
             dma((5,)),
-            dma((4,)),
+            dma((6,)),
             dma((arrays, groups - 1)),
             dma((groups,)),
             dma((groups,)),
@@ -371,62 +398,274 @@
     )
 
 
-def serve_body(served, scaled, got, gate_ref, up_ref, down_ref, mixed_ref, mixed, sem):
-    arrays, parts, _, wide = served.shape
-    rows = got.shape[2]
+def store_body(wide, down, gate_ref, up_ref, down_ref, token_ref, sem):
+    parts, width, hold = down.shape
     hidden = FF // parts
+    groups, per = lax.axis_size("fs"), hold // hidden
+    rows = width // groups
     f = lax.axis_index("fs")
-    outs = (gate_ref, up_ref, down_ref)
+    _, odds, evens = block_order(groups)
+
+    def put(k):
+        at = pl.ds(pl.multiple_of(jnp.bitwise_xor(f, k) * rows, rows), rows)
+        for i in range(parts):
+            for e in range(per):
+                pltpu.make_async_copy(
+                    down.at[i, at, pl.ds(e * hidden, hidden)],
+                    down_ref.at[at, pl.ds(e * FF + i * hidden, hidden)],
+                    sem.at[2],
+                ).start()
+
+    def wait(count):
+        done = down_ref.at[pl.ds(0, count * rows)]
+        pltpu.make_async_copy(done, done, sem.at[2]).wait()
+
+    outs = (gate_ref, up_ref)
     for w, out in enumerate(outs):
         for i in range(parts):
-            for e in range(wide // hidden):
+            for e in range(per):
                 pltpu.make_async_copy(
-                    served.at[w, i, :, pl.ds(e * hidden, hidden)],
+                    wide.at[w, i, :, pl.ds(e * hidden, hidden)],
                     out.at[:, pl.ds(e * FF + i * hidden, hidden)],
                     sem.at[w],
                 ).start()
-    total = None
-    for i in range(parts):
-        term = lax.dot_general(
-            scaled[i],
-            served[2, i, pl.ds(pl.multiple_of(f * rows, rows), rows), :],
-            (((1,), (1,)), ((), ())),
-            preferred_element_type=jnp.float32,
-        )
-        total = term if total is None else total + term
-    for k in range(got.shape[0]):
-        total = total + got[k].astype(jnp.float32)
-    mixed[...] = (total * FF ** (-0.5)).astype(jnp.bfloat16)
-    final = pltpu.make_async_copy(mixed, mixed_ref, sem.at[arrays])
-    final.start()
+    for k in odds:
+        put(k)
+
+    @pl.when(f % 2 == 1)
+    def _():
+        for k in evens:
+            put(k)
+        wait(groups)
+
+    @pl.when(f % 2 == 0)
+    def _():
+        wait(len(odds))
+
     for w, out in enumerate(outs):
         pltpu.make_async_copy(out, out, sem.at[w]).wait()
-    final.wait()
-
-
-def serve(served, scaled, got):
-    arrays, parts, width, wide = served.shape
-    _, tokens, rows = got.shape
-    out = jax.ShapeDtypeStruct((width, parts * wide), served.dtype)
+
+
+def hold_in_vmem(*arrays):
+    return [pltpu.with_memory_space_constraint(one, pltpu.VMEM) for one in arrays]
+
+
+def store(wide, down):
+    parts, width, hold = down.shape
+    out = pltpu.HBM((width, parts * hold), down.dtype)
+    vmem, hbm = pl.BlockSpec(memory_space=pltpu.VMEM), pl.BlockSpec(memory_space=pltpu.HBM)
+    return pl.pallas_call(
+        store_body,
+        in_specs=[vmem, vmem],
+        out_specs=[hbm, hbm, hbm, hbm],
+        out_shape=[out, out, out, pltpu.HBM((8, 128), jnp.float32)],
+        scratch_shapes=[pltpu.SemaphoreType.DMA((3,))],
+        compiler_params=pltpu.CompilerParams(vmem_limit_bytes=4 * 1024 * 1024),
+        name="store",
+    )(*hold_in_vmem(wide, down))
+
+
+def finish_body(down, scaled, got, token_ref, late, got_late, mine, part, send_sem, xr, yr, dr, pr):
+    f, t = lax.axis_index("fs"), lax.axis_index("tp")
+    tx, ty = jnp.bitwise_xor(t, 1), jnp.bitwise_xor(t, 2)
+    parts = down.shape[0]
+    rows = late.shape[2]
+    half, quarter = rows // 2, rows // 4
+    _, odds, evens = block_order(lax.axis_size("fs"))
+    count = len(evens)
+
+    def own(i, begin=0, size=rows):
+        first = jnp.bitwise_xor(f, evens[i]) * rows + begin
+        return down.at[t, pl.ds(pl.multiple_of(first, size), size)]
+
+    def landed(j, q, begin=0, size=half):
+        return late.at[j, q // 2, pl.ds(q % 2 * half + begin, size)]
+
+    def x_copy(q):
+        source = own(q // 2, q % 2 * half, half)
+        return remote(source, landed(0, q), send_sem.at[0], xr.at[q], {"fs": f, "tp": tx})
+
+    def y_copy(q):
+        source = own(q // 2, q % 2 * half, half)
+        return remote(source, landed(1, q), send_sem.at[1], yr.at[q], {"fs": f, "tp": ty})
+
+    def to_y(q):
+        source, target = landed(0, q, 0, quarter), landed(2, q, 0, quarter)
+        return remote(source, target, send_sem.at[1], dr.at[q], {"fs": f, "tp": ty})
+
+    def to_x(q):
+        source, target = landed(1, q, quarter, quarter), landed(2, q, quarter, quarter)
+        return remote(source, target, send_sem.at[0], dr.at[q], {"fs": f, "tp": tx})
+
+    def side_start(q):
+        x_copy(q).start()
+        y_copy(q).start()
+
+    def forward(q):
+        x_copy(q).wait_recv()
+        to_y(q).start()
+        y_copy(q).wait_recv()
+        to_x(q).start()
+
+    def straight(i):
+        total = matmul_nt(scaled[t], own(i)[...])
+        for j in (1, 2):
+            total = total + matmul_nt(scaled[jnp.bitwise_xor(t, j)], late[j - 1, i])
+        return total
+
+    def diagonal(i):
+        for q in (2 * i, 2 * i + 1):
+            one = landed(2, q)
+            remote(one, one, send_sem.at[0], dr.at[q], {"fs": f, "tp": tx}).wait_recv()
+        return matmul_nt(scaled[jnp.bitwise_xor(t, 3)], late[2, i])
+
+    def features(i):
+        mine[...] = straight(i)
+        part[i] = (mine[...] + diagonal(i)).astype(jnp.bfloat16)
+        device = {"fs": jnp.bitwise_xor(f, evens[i]), "tp": t}
+        remote(part.at[i], got_late.at[i], send_sem.at[2], pr, device).start()
+
+    def collected(total, chosen):
+        for k in chosen:
+            total = total + got[k - 1].astype(jnp.float32)
+        return total
+
+    def run():
+        ahead, chunks = 4, 2 * count
+        for q in range(ahead):
+            side_start(q)
+        sent = ahead
+        for q in range(chunks):
+            forward(q)
+            if sent < chunks - 2 or (q % 2 == 1 and sent < chunks):
+                side_start(sent)
+                sent += 1
+            if q % 2 == 1 and 3 <= q < chunks - 1:
+                features((q - 3) // 2)
+            if q == chunks - 2:
+                features(count - 2)
+        mine[...] = collected(straight(count - 1), odds)
+        mine[...] += diagonal(count - 1)
+        sides = late.at[:, :, pl.ds(0, half)]
+        for i, whole in enumerate((sides, sides, part)):
+            remote(whole, whole, send_sem.at[i], pr, {"fs": f, "tp": tx}).wait_send()
+        remote(got_late, got_late, send_sem.at[2], pr, {"fs": f, "tp": tx}).wait_recv()
+
+    @pl.when(f % 2 == 0)
+    def _():
+        barrier = pltpu.get_barrier_semaphore()
+        others = [{"fs": jnp.bitwise_xor(f, k), "tp": t} for k in evens[:-1]]
+        others += [{"fs": f, "tp": tx}, {"fs": f, "tp": ty}]
+        for other in others:
+            pl.semaphore_signal(barrier, inc=1, device_id=other, device_id_type=MESH)
+        pl.semaphore_wait(barrier, len(others))
+        run()
+
+    @pl.when(f % 2 == 1)
+    def _():
+        at = pl.ds(pl.multiple_of(f * rows, rows), rows)
+        total = matmul_nt(scaled[0], down[0, at, :])
+        for i in range(1, parts):
+            total = total + matmul_nt(scaled[i], down[i, at, :])
+        mine[...] = collected(total, odds + evens[:-1])
+
+
+def finish(down, scaled, got, token, groups):
+    parts, width, hold = down.shape
+    tokens, rows, count = scaled.shape[1], width // groups, groups // 2
+    vmem, hbm = pl.BlockSpec(memory_space=pltpu.VMEM), pl.BlockSpec(memory_space=pltpu.HBM)
+    dma = pltpu.SemaphoreType.DMA
+    return pl.pallas_call(
+        finish_body,
+        in_specs=[vmem, vmem, vmem, hbm],
+        out_specs=[vmem, vmem, vmem],
+        out_shape=[
+            pltpu.VMEM((parts - 1, count, rows, hold), down.dtype),
+            pltpu.VMEM((count - 1, tokens, rows), jnp.bfloat16),
+            pltpu.VMEM((tokens, rows), jnp.float32),
+        ],
+        scratch_shapes=[
+            pltpu.VMEM((count - 1, tokens, rows), jnp.bfloat16),
+            dma((3,)),
+            dma((2 * count,)),
+            dma((2 * count,)),
+            dma((2 * count,)),
+            dma,
+        ],
+        compiler_params=pltpu.CompilerParams(
+            collective_id=1, has_side_effects=True, vmem_limit_bytes=4 * 1024 * 1024
+        ),
+        name="finish",
+    )(*hold_in_vmem(down, scaled, got), pltpu.with_memory_space_constraint(token, pltpu.HBM))
+
+
+def serve_body(down, late, got_late, mine, down_in, down_ref, mixed_ref, mixed, sem):
+    parts, width, hold = down.shape
+    hidden, rows = FF // parts, late.shape[2]
+    f, t = lax.axis_index("fs"), lax.axis_index("tp")
+    _, _, evens = block_order(width // rows)
+    count = len(evens)
+
+    def put(i):
+        at = pl.ds(pl.multiple_of(jnp.bitwise_xor(f, evens[i]) * rows, rows), rows)
+        for j in range(parts):
+            origin = jnp.bitwise_xor(t, j)
+            source = late.at[j - 1, i] if j > 0 else down.at[t, at]
+            for e in range(hold // hidden):
+                begin = pl.multiple_of(e * FF + origin * hidden, hidden)
+                pltpu.make_async_copy(
+                    source.at[:, pl.ds(e * hidden, hidden)], down_ref.at[at, pl.ds(begin, hidden)], sem.at[0]
+                ).start()
+
+    def finish_mixed(total):
+        mixed[...] = (total * FF ** (-0.5)).astype(jnp.bfloat16)
+        final = pltpu.make_async_copy(mixed, mixed_ref, sem.at[1])
+        final.start()
+        return final
+
+    @pl.when(f % 2 == 0)
+    def _():
+        for i in range(count):
+            put(i)
+        total = mine[...]
+        for i in range(count - 1):
+            total = total + got_late[i].astype(jnp.float32)
+        final = finish_mixed(total)
+        done = down_ref.at[pl.ds(0, count * rows)]
+        pltpu.make_async_copy(done, done, sem.at[0]).wait()
+        final.wait()
+
+    @pl.when(f % 2 == 1)
+    def _():
+        finish_mixed(mine[...]).wait()
+
+
+def serve(down, late, got_late, mine, down_out):
+    tokens, rows = mine.shape
     vmem, hbm = pl.BlockSpec(memory_space=pltpu.VMEM), pl.BlockSpec(memory_space=pltpu.HBM)
     return pl.pallas_call(
         serve_body,
-        in_specs=[vmem, vmem, vmem],
-        out_specs=[hbm, hbm, hbm, hbm],
-        out_shape=[out, out, out, jax.ShapeDtypeStruct((tokens, rows), jnp.bfloat16)],
-        scratch_shapes=[pltpu.VMEM((tokens, rows), jnp.bfloat16), pltpu.SemaphoreType.DMA((arrays + 1,))],
+        in_specs=[vmem] * 4 + [hbm],
+        out_specs=[hbm, hbm],
+        out_shape=[pltpu.HBM(down_out.shape, down_out.dtype), pltpu.HBM((tokens, rows), jnp.bfloat16)],
+        input_output_aliases={4: 0},
+        scratch_shapes=[pltpu.VMEM((tokens, rows), jnp.bfloat16), pltpu.SemaphoreType.DMA((2,))],
         compiler_params=pltpu.CompilerParams(vmem_limit_bytes=4 * 1024 * 1024),
         name="serve",
-    )(*[pltpu.with_memory_space_constraint(one, pltpu.VMEM) for one in (served, scaled, got)])
+    )(*hold_in_vmem(down, late, got_late, mine), pltpu.with_memory_space_constraint(down_out, pltpu.HBM))
 
 
 def direct_shards(
     prompt, norm_gain, gate_master, up_master, down_master, group_choice, inner_choice, route_weight
 ):
-    served, scaled, got = spread(
+    groups = lax.axis_size("fs")
+    wide, down, scaled, got = spread(
         prompt, norm_gain, gate_master, up_master, down_master, group_choice, inner_choice, route_weight
     )
-    return tuple(serve(served, scaled, got))
+    gate_local, up_local, down_some, token = store(wide, down)
+    late, got_late, mine = finish(down, scaled, got, token, groups)
+    down_local, mixed = serve(down, late, got_late, mine, down_some)
+    return (gate_local, up_local, down_local, mixed)
 
 
 def fits_direct(mesh):

time: 220 us -> 216 us (0.982)
  the two profiles are of different devices: /device:TPU:1 before, /device:TPU:0 now
where the time goes in v2:
time: 216 us; the launch traced here: 215 us
  Pallas kernels  215 us (100%)
    pallas_call x1, Pallas kernels, spread(): pl.pallas_call(spread_body, in_specs=[pl.BlockSpec(memory_space=pltpu.HBM...  181 us
    pallas_call x1, Pallas kernels, finish(): pl.pallas_call(finish_body, in_specs=[vmem, vmem, vmem, hbm], out_specs=[...  24.8 us
    pallas_call x1, Pallas kernels, store(): pl.pallas_call(store_body, in_specs=[vmem, vmem], out_specs=[hbm, hbm, hb...  7.04 us

profile of v2, /device:TPU:0, one launch (start us, length us, event | category | flops | bytes accessed | tf_op | source)
XLA Modules:
  0.0 215.5 jit_solution(5992008749692746681)
XLA Ops:
  0.6 181.0 %spread.1 = (bf16[2,4,2048,512]{3,2,1,0:T(8,128)(2,1)S(1)}, bf16[4,2048,512]{2,1,0:T(8,128)(2,1)S(1)}, bf16[4,256,512]{2,1,0:T(8,128)(2,1)S(1)}, bf16[7,256,256]{2,1,0:T(8,128)(2,1)S(1)}) custom-call(f32[1,256]{1,0:T(1,128)} %bitcast.12, f32[8,4,256,128]{3,2,1,0:T(8,128)} %bitcast.7, f32[8,4,256,128]{3,2,1,0:T(8,128)} %bitcast.8, ...), custom_call_target="tpu_custom_call" | custom-call | tf_op jit(solution)/shard_map/spread/pallas_call | solution.py:355
  181.6 7.0 %store.1 = (bf16[2048,2048]{1,0:T(8,128)(2,1)}, bf16[2048,2048]{1,0:T(8,128)(2,1)}, bf16[2048,2048]{1,0:T(8,128)(2,1)}, f32[8,128]{1,0:T(8,128)}) custom-call(bf16[2,4,2048,512]{3,2,1,0:T(8,128)(2,1)S(1)} %get-tuple-element.17.wide, bf16[4,2048,512]{2,1,0:T(8,128)(2,1)S(1)} %get-tuple-element.18.down), custom_call_target="tpu_custom_call" | custom-call | tf_op jit(solution)/shard_map/store/pallas_call | solution.py:457
  188.7 24.8 %finish.1 = (bf16[3,4,256,512]{3,2,1,0:T(8,128)(2,1)S(1)}, bf16[3,256,256]{2,1,0:T(8,128)(2,1)S(1)}, f32[256,256]{1,0:T(8,128)S(1)}) custom-call(bf16[4,2048,512]{2,1,0:T(8,128)(2,1)S(1)} %get-tuple-element.18.down, bf16[4,256,512]{2,1,0:T(8,128)(2,1)S(1)} %get-tuple-element.21.scaled, bf16[7,256,256]{2,1,0:T(8,128)(2,1)S(1)} %get-tuple-element.22.got, ...), custom_call_target="tpu_custom_call" | custom-call | tf_op jit(solution)/shard_map/finish/pallas_call | solution.py:578
  213.4 2.0 serve.1

commit v3 on v2

--- a/solution.py
+++ b/solution.py
@@ -199,6 +199,11 @@
         x_copy(s, t).start()
         y_copy(s, t).start()
 
+    def side_half(s, begin):
+        one = block(order[s][0], t, order[s][1], begin, half)
+        remote(one, one, send_sem.at[s // base], xr.at[s % groups], {"fs": f, "tp": tx}).start()
+        remote(one, one, send_sem.at[2 + s // base], yr.at[s % groups], {"fs": f, "tp": ty}).start()
+
     def forward(s):
         x_copy(s, tx).wait_recv()
         to_y(s).start()
@@ -261,20 +266,20 @@
         pl.semaphore_signal(barrier, inc=1, device_id={"fs": peer(k), "tp": t}, device_id_type=MESH)
     for other in (tx, ty):
         pl.semaphore_signal(barrier, inc=1, device_id={"fs": f, "tp": other}, device_id_type=MESH)
+    small[0].wait()
+    scale[...] = jnp.broadcast_to(gain[...], (hidden, rows)).T
+    load(0).wait()
+    put(0, 0, block(0, t, 0))
     for k in near[1:]:
         load(k).start()
     for w in (1, 2):
         bulk(w).start()
     for copy in small[1:]:
         copy.start()
-    small[0].wait()
-    scale[...] = jnp.broadcast_to(gain[...], (hidden, rows)).T
-    load(0).wait()
-    put(0, 0, block(0, t, 0))
+    pl.semaphore_wait(barrier, groups + 1)
+    side_start(0)
     load(near[1]).wait()
     put(0, near[1], cast.at[0, near[1] - 1])
-    pl.semaphore_wait(barrier, groups + 1)
-    side_start(0)
     for before, k in zip(near[1:], near[2:]):
         load(k).wait()
         put(0, k, cast.at[0, k - 1])
@@ -289,8 +294,16 @@
         if s > 0:
             if k > 0:
                 z_arrival(w, k).wait_recv()
-            side_start(s)
-            forward(s - 1)
+            if s == split:
+                side_half(s, 0)
+                forward(s - 1)
+                side_half(s, half)
+            else:
+                side_start(s)
+            if s == split + 1:
+                features(s - 2)
+            if s != split:
+                forward(s - 1)
         for at, array, one in sends:
             if at == s:
                 z_copy(array, one).start()
@@ -309,7 +322,7 @@
         if s == base + 2:
             diagonal_wait(base - 1)
             hidden_units(td)
-        if s >= base + 2:
+        if s >= base + 2 and s != split + 1:
             features(s - 2)
 
     def drain(end):
@@ -331,13 +344,13 @@
     for s in range(split):
         step(s)
 
-    @pl.when(f % 2 == 0)
+    @pl.when(f % 2 == 1)
     def _():
         for k in evens[:-1]:
             z_arrival(2, k).wait_recv()
         drain(split)
 
-    @pl.when(f % 2 == 1)
+    @pl.when(f % 2 == 0)
     def _():
         for s in range(split, len(order)):
             step(s)
@@ -432,13 +445,13 @@
     for k in odds:
         put(k)
 
-    @pl.when(f % 2 == 1)
+    @pl.when(f % 2 == 0)
     def _():
         for k in evens:
             put(k)
         wait(groups)
 
-    @pl.when(f % 2 == 0)
+    @pl.when(f % 2 == 1)
     def _():
         wait(len(odds))
 
@@ -478,23 +491,30 @@
         first = jnp.bitwise_xor(f, evens[i]) * rows + begin
         return down.at[t, pl.ds(pl.multiple_of(first, size), size)]
 
-    def landed(j, q, begin=0, size=half):
-        return late.at[j, q // 2, pl.ds(q % 2 * half + begin, size)]
+    pieces = [(i, c * half, half) for i in range(count) for c in range(2)]
+    pieces[-1:] = [(count - 1, half, quarter), (count - 1, half + quarter, quarter)]
+
+    def landed(j, q, which=None):
+        i, begin, size = pieces[q]
+        if which is not None:
+            size = size // 2
+            begin = begin + which * size
+        return late.at[j, i, pl.ds(begin, size)]
 
     def x_copy(q):
-        source = own(q // 2, q % 2 * half, half)
+        source = own(*pieces[q])
         return remote(source, landed(0, q), send_sem.at[0], xr.at[q], {"fs": f, "tp": tx})
 
     def y_copy(q):
-        source = own(q // 2, q % 2 * half, half)
+        source = own(*pieces[q])
         return remote(source, landed(1, q), send_sem.at[1], yr.at[q], {"fs": f, "tp": ty})
 
     def to_y(q):
-        source, target = landed(0, q, 0, quarter), landed(2, q, 0, quarter)
+        source, target = landed(0, q, 0), landed(2, q, 0)
         return remote(source, target, send_sem.at[1], dr.at[q], {"fs": f, "tp": ty})
 
     def to_x(q):
-        source, target = landed(1, q, quarter, quarter), landed(2, q, quarter, quarter)
+        source, target = landed(1, q, 1), landed(2, q, 1)
         return remote(source, target, send_sem.at[0], dr.at[q], {"fs": f, "tp": tx})
 
     def side_start(q):
@@ -514,7 +534,7 @@
         return total
 
     def diagonal(i):
-        for q in (2 * i, 2 * i + 1):
+        for q in [q for q, piece in enumerate(pieces) if piece[0] == i]:
             one = landed(2, q)
             remote(one, one, send_sem.at[0], dr.at[q], {"fs": f, "tp": tx}).wait_recv()
         return matmul_nt(scaled[jnp.bitwise_xor(t, 3)], late[2, i])
@@ -531,18 +551,18 @@
         return total
 
     def run():
-        ahead, chunks = 4, 2 * count
-        for q in range(ahead):
-            side_start(q)
-        sent = ahead
-        for q in range(chunks):
-            forward(q)
-            if sent < chunks - 2 or (q % 2 == 1 and sent < chunks):
+        total, sent = len(pieces), 0
+        for q in range(total):
+            goal = 4 if q == 0 else 5 + q // 2
+            if q >= 2 * count - 2:
+                goal = total
+            while sent < min(goal, total):
                 side_start(sent)
                 sent += 1
-            if q % 2 == 1 and 3 <= q < chunks - 1:
-                features((q - 3) // 2)
-            if q == chunks - 2:
+            if q >= 4 and q % 2 == 0 and q < 2 * count - 1:
+                features(q // 2 - 2)
+            forward(q)
+            if q == 2 * count - 2:
                 features(count - 2)
         mine[...] = collected(straight(count - 1), odds)
         mine[...] += diagonal(count - 1)
@@ -551,7 +571,7 @@
             remote(whole, whole, send_sem.at[i], pr, {"fs": f, "tp": tx}).wait_send()
         remote(got_late, got_late, send_sem.at[2], pr, {"fs": f, "tp": tx}).wait_recv()
 
-    @pl.when(f % 2 == 0)
+    @pl.when(f % 2 == 1)
     def _():
         barrier = pltpu.get_barrier_semaphore()
         others = [{"fs": jnp.bitwise_xor(f, k), "tp": t} for k in evens[:-1]]
@@ -561,7 +581,7 @@
         pl.semaphore_wait(barrier, len(others))
         run()
 
-    @pl.when(f % 2 == 1)
+    @pl.when(f % 2 == 0)
     def _():
         at = pl.ds(pl.multiple_of(f * rows, rows), rows)
         total = matmul_nt(scaled[0], down[0, at, :])
@@ -587,9 +607,9 @@
         scratch_shapes=[
             pltpu.VMEM((count - 1, tokens, rows), jnp.bfloat16),
             dma((3,)),
-            dma((2 * count,)),
-            dma((2 * count,)),
-            dma((2 * count,)),
+            dma((2 * count + 1,)),
+            dma((2 * count + 1,)),
+            dma((2 * count + 1,)),
             dma,
         ],
         compiler_params=pltpu.CompilerParams(
@@ -623,7 +643,7 @@
         final.start()
         return final
 
-    @pl.when(f % 2 == 0)
+    @pl.when(f % 2 == 1)
     def _():
         for i in range(count):
             put(i)
@@ -635,7 +655,7 @@
         pltpu.make_async_copy(done, done, sem.at[0]).wait()
         final.wait()
 
-    @pl.when(f % 2 == 1)
+    @pl.when(f % 2 == 0)
     def _():
         finish_mixed(mine[...]).wait()
 

time: 216 us -> 214 us (level)
  the two profiles are of different devices: /device:TPU:0 before, /device:TPU:1 now
where the time goes in v3:
time: 214 us
  Pallas kernels  213 us (100%)
    pallas_call x1, Pallas kernels, spread(): pl.pallas_call(spread_body, in_specs=[pl.BlockSpec(memory_space=pltpu.HBM...  180 us
    pallas_call x1, Pallas kernels, finish(): pl.pallas_call(finish_body, in_specs=[vmem, vmem, vmem, hbm], out_specs=[...  24.1 us
    pallas_call x1, Pallas kernels, store(): pl.pallas_call(store_body, in_specs=[vmem, vmem], out_specs=[hbm, hbm, hb...  7.04 us

profile of v3, /device:TPU:1, one launch (start us, length us, event | category | flops | bytes accessed | tf_op | source)
XLA Modules:
  0.0 213.6 jit_solution(3947561371656097279)
XLA Ops:
  0.6 179.8 %spread.1 = (bf16[2,4,2048,512]{3,2,1,0:T(8,128)(2,1)S(1)}, bf16[4,2048,512]{2,1,0:T(8,128)(2,1)S(1)}, bf16[4,256,512]{2,1,0:T(8,128)(2,1)S(1)}, bf16[7,256,256]{2,1,0:T(8,128)(2,1)S(1)}) custom-call(f32[1,256]{1,0:T(1,128)} %bitcast.12, f32[8,4,256,128]{3,2,1,0:T(8,128)} %bitcast.7, f32[8,4,256,128]{3,2,1,0:T(8,128)} %bitcast.8, ...), custom_call_target="tpu_custom_call" | custom-call | tf_op jit(solution)/shard_map/spread/pallas_call | solution.py:368
  180.4 7.0 %store.1 = (bf16[2048,2048]{1,0:T(8,128)(2,1)}, bf16[2048,2048]{1,0:T(8,128)(2,1)}, bf16[2048,2048]{1,0:T(8,128)(2,1)}, f32[8,128]{1,0:T(8,128)}) custom-call(bf16[2,4,2048,512]{3,2,1,0:T(8,128)(2,1)S(1)} %get-tuple-element.17.wide, bf16[4,2048,512]{2,1,0:T(8,128)(2,1)S(1)} %get-tuple-element.18.down), custom_call_target="tpu_custom_call" | custom-call | tf_op jit(solution)/shard_map/store/pallas_call | solution.py:470
  187.5 24.1 %finish.1 = (bf16[3,4,256,512]{3,2,1,0:T(8,128)(2,1)S(1)}, bf16[3,256,256]{2,1,0:T(8,128)(2,1)S(1)}, f32[256,256]{1,0:T(8,128)S(1)}) custom-call(bf16[4,2048,512]{2,1,0:T(8,128)(2,1)S(1)} %get-tuple-element.18.down, bf16[4,256,512]{2,1,0:T(8,128)(2,1)S(1)} %get-tuple-element.21.scaled, bf16[7,256,256]{2,1,0:T(8,128)(2,1)S(1)} %get-tuple-element.22.got, ...), custom_call_target="tpu_custom_call" | custom-call | tf_op jit(solution)/shard_map/finish/pallas_call | solution.py:598
  211.6 2.0 serve.1

commit v4 on v3

--- a/solution.py
+++ b/solution.py
@@ -129,6 +129,7 @@
     yr,
     dr,
     pr,
+    column_in,
 ):
     f, t = lax.axis_index("fs"), lax.axis_index("tp")
     tx, ty, td = jnp.bitwise_xor(t, 1), jnp.bitwise_xor(t, 2), jnp.bitwise_xor(t, 3)
@@ -262,8 +263,20 @@
     small[0].start()
     load(0).start()
     barrier = pltpu.get_barrier_semaphore()
-    for k in range(1, groups):
-        pl.semaphore_signal(barrier, inc=1, device_id={"fs": peer(k), "tp": t}, device_id_type=MESH)
+
+    def greet(chosen):
+        for k in chosen:
+            device = {"fs": peer(k), "tp": t}
+            pl.semaphore_signal(barrier, inc=1, device_id=device, device_id_type=MESH)
+
+    @pl.when(f % 2 == 0)
+    def _():
+        greet([1] + list(range(2, groups, 2)))
+
+    @pl.when(f % 2 == 1)
+    def _():
+        greet(range(1, groups, 2))
+
     for other in (tx, ty):
         pl.semaphore_signal(barrier, inc=1, device_id={"fs": f, "tp": other}, device_id_type=MESH)
     small[0].wait()
@@ -276,10 +289,19 @@
         bulk(w).start()
     for copy in small[1:]:
         copy.start()
-    pl.semaphore_wait(barrier, groups + 1)
+    pl.semaphore_wait(barrier, 3 + (groups - 2) * (1 - f % 2))
     side_start(0)
     load(near[1]).wait()
     put(0, near[1], cast.at[0, near[1] - 1])
+
+    @pl.when(f % 2 == 0)
+    def _():
+        pl.semaphore_signal(column_in, inc=1, device_id={"fs": peer(1), "tp": t}, device_id_type=MESH)
+
+    @pl.when(f % 2 == 1)
+    def _():
+        pl.semaphore_wait(column_in, 1)
+
     for before, k in zip(near[1:], near[2:]):
         load(k).wait()
         put(0, k, cast.at[0, k - 1])
@@ -396,6 +418,7 @@
             dma((groups,)),
             dma((groups,)),
             dma,
+            pltpu.SemaphoreType.REGULAR,
         ],
         compiler_params=pltpu.CompilerParams(
             collective_id=0, has_side_effects=True, vmem_limit_bytes=32 * 1024 * 1024

time: 214 us -> 212 us (level)
    pallas_call x1, Pallas kernels: 180 us -> 178 us  [spread(): pl.pallas_call(spread_body, in_specs=[pl.BlockSpec(memory_space=pltpu.HBM...]
where the time goes in v4:
time: 212 us; the launch traced here: 211 us
  Pallas kernels  211 us (100%)
    pallas_call x1, Pallas kernels, spread(): pl.pallas_call(spread_body, in_specs=[pl.BlockSpec(memory_space=pltpu.HBM...  178 us
    pallas_call x1, Pallas kernels, finish(): pl.pallas_call(finish_body, in_specs=[vmem, vmem, vmem, hbm], out_specs=[...  24.2 us
    pallas_call x1, Pallas kernels, store(): pl.pallas_call(store_body, in_specs=[vmem, vmem], out_specs=[hbm, hbm, hb...  7.04 us

profile of v4, /device:TPU:1, one launch (start us, length us, event | category | flops | bytes accessed | tf_op | source)
XLA Modules:
  0.0 211.5 jit_solution(14376069750235857689)
XLA Ops:
  0.6 177.5 %spread.1 = (bf16[2,4,2048,512]{3,2,1,0:T(8,128)(2,1)S(1)}, bf16[4,2048,512]{2,1,0:T(8,128)(2,1)S(1)}, bf16[4,256,512]{2,1,0:T(8,128)(2,1)S(1)}, bf16[7,256,256]{2,1,0:T(8,128)(2,1)S(1)}) custom-call(f32[1,256]{1,0:T(1,128)} %bitcast.12, f32[8,4,256,128]{3,2,1,0:T(8,128)} %bitcast.7, f32[8,4,256,128]{3,2,1,0:T(8,128)} %bitcast.8, ...), custom_call_target="tpu_custom_call" | custom-call | tf_op jit(solution)/shard_map/spread/pallas_call | solution.py:390
  178.2 7.0 %store.1 = (bf16[2048,2048]{1,0:T(8,128)(2,1)}, bf16[2048,2048]{1,0:T(8,128)(2,1)}, bf16[2048,2048]{1,0:T(8,128)(2,1)}, f32[8,128]{1,0:T(8,128)}) custom-call(bf16[2,4,2048,512]{3,2,1,0:T(8,128)(2,1)S(1)} %get-tuple-element.17.wide, bf16[4,2048,512]{2,1,0:T(8,128)(2,1)S(1)} %get-tuple-element.18.down), custom_call_target="tpu_custom_call" | custom-call | tf_op jit(solution)/shard_map/store/pallas_call | solution.py:493
  185.2 24.2 %finish.1 = (bf16[3,4,256,512]{3,2,1,0:T(8,128)(2,1)S(1)}, bf16[3,256,256]{2,1,0:T(8,128)(2,1)S(1)}, f32[256,256]{1,0:T(8,128)S(1)}) custom-call(bf16[4,2048,512]{2,1,0:T(8,128)(2,1)S(1)} %get-tuple-element.18.down, bf16[4,256,512]{2,1,0:T(8,128)(2,1)S(1)} %get-tuple-element.21.scaled, bf16[7,256,256]{2,1,0:T(8,128)(2,1)S(1)} %get-tuple-element.22.got, ...), custom_call_target="tpu_custom_call" | custom-call | tf_op jit(solution)/shard_map/finish/pallas_call | solution.py:621
  209.4 2.0 serve.1

commit v5 on v4

--- a/solution.py
+++ b/solution.py
@@ -308,8 +308,17 @@
         z_copy(0, before).start()
     z_copy(0, near[-1]).start()
 
-    sends = [(lag if i < 3 else lag + (i + 1) // 2, 1, k) for i, k in enumerate(near[1:])]
-    sends += [(groups + 3 + i // 2, 2, k) for i, k in enumerate(near[:0:-1])]
+    near_sends = [(lag, 1, k) for k in near[1:4]] + [(groups + 5, 2, k) for k in near[1:4]]
+    far = {1: near[4:], 2: [k for k in odds + evens if k >= 4]}
+    inner_sends = [(lag + 2 + i // 2, 1, k) for i, k in enumerate(far[1])]
+    inner_sends += [(groups + 4, 2, k) for k in far[2]]
+    outer_sends = [(groups + 1, 1, k) for k in far[1]] + [(groups + 7, 2, k) for k in far[2]]
+    outer = (f // 2 == 0) | (f // 2 == groups // 2 - 1)
+
+    def send_at(s, chosen):
+        for at, array, one in chosen:
+            if at == s:
+                z_copy(array, one).start()
 
     def step(s):
         w, k = order[s]
@@ -326,9 +335,11 @@
                 features(s - 2)
             if s != split:
                 forward(s - 1)
-        for at, array, one in sends:
-            if at == s:
-                z_copy(array, one).start()
+        send_at(s, near_sends)
+        if any(at == s for at, _, _ in inner_sends):
+            pl.when(jnp.logical_not(outer))(lambda: send_at(s, inner_sends))
+        if any(at == s for at, _, _ in outer_sends):
+            pl.when(outer)(lambda: send_at(s, outer_sends))
         if s < 2:
             put_all(s + 1)
         if s == groups:
@@ -534,11 +545,11 @@
 
     def to_y(q):
         source, target = landed(0, q, 0), landed(2, q, 0)
-        return remote(source, target, send_sem.at[1], dr.at[q], {"fs": f, "tp": ty})
+        return remote(source, target, send_sem.at[1], dr.at[pieces[q][0]], {"fs": f, "tp": ty})
 
     def to_x(q):
         source, target = landed(1, q, 1), landed(2, q, 1)
-        return remote(source, target, send_sem.at[0], dr.at[q], {"fs": f, "tp": tx})
+        return remote(source, target, send_sem.at[0], dr.at[pieces[q][0]], {"fs": f, "tp": tx})
 
     def side_start(q):
         x_copy(q).start()
@@ -556,15 +567,15 @@
             total = total + matmul_nt(scaled[jnp.bitwise_xor(t, j)], late[j - 1, i])
         return total
 
-    def diagonal(i):
-        for q in [q for q, piece in enumerate(pieces) if piece[0] == i]:
-            one = landed(2, q)
-            remote(one, one, send_sem.at[0], dr.at[q], {"fs": f, "tp": tx}).wait_recv()
-        return matmul_nt(scaled[jnp.bitwise_xor(t, 3)], late[2, i])
+    def diagonal_wait(i):
+        one = late.at[2, i]
+        remote(one, one, send_sem.at[0], dr.at[i], {"fs": f, "tp": tx}).wait_recv()
 
     def features(i):
         mine[...] = straight(i)
-        part[i] = (mine[...] + diagonal(i)).astype(jnp.bfloat16)
+        diagonal_wait(i)
+        total = mine[...] + matmul_nt(scaled[jnp.bitwise_xor(t, 3)], late[2, i])
+        part[i] = total.astype(jnp.bfloat16)
         device = {"fs": jnp.bitwise_xor(f, evens[i]), "tp": t}
         remote(part.at[i], got_late.at[i], send_sem.at[2], pr, device).start()
 
@@ -588,7 +599,7 @@
             if q == 2 * count - 2:
                 features(count - 2)
         mine[...] = collected(straight(count - 1), odds)
-        mine[...] += diagonal(count - 1)
+        diagonal_wait(count - 1)
         sides = late.at[:, :, pl.ds(0, half)]
         for i, whole in enumerate((sides, sides, part)):
             remote(whole, whole, send_sem.at[i], pr, {"fs": f, "tp": tx}).wait_send()
@@ -632,7 +643,7 @@
             dma((3,)),
             dma((2 * count + 1,)),
             dma((2 * count + 1,)),
-            dma((2 * count + 1,)),
+            dma((count,)),
             dma,
         ],
         compiler_params=pltpu.CompilerParams(
@@ -642,7 +653,7 @@
     )(*hold_in_vmem(down, scaled, got), pltpu.with_memory_space_constraint(token, pltpu.HBM))
 
 
-def serve_body(down, late, got_late, mine, down_in, down_ref, mixed_ref, mixed, sem):
+def serve_body(down, late, scaled, got_late, mine, down_in, down_ref, mixed_ref, mixed, sem):
     parts, width, hold = down.shape
     hidden, rows = FF // parts, late.shape[2]
     f, t = lax.axis_index("fs"), lax.axis_index("tp")
@@ -670,7 +681,7 @@
     def _():
         for i in range(count):
             put(i)
-        total = mine[...]
+        total = mine[...] + matmul_nt(scaled[jnp.bitwise_xor(t, 3)], late[2, count - 1])
         for i in range(count - 1):
             total = total + got_late[i].astype(jnp.float32)
         final = finish_mixed(total)
@@ -683,19 +694,19 @@
         finish_mixed(mine[...]).wait()
 
 
-def serve(down, late, got_late, mine, down_out):
+def serve(down, late, scaled, got_late, mine, down_out):
     tokens, rows = mine.shape
     vmem, hbm = pl.BlockSpec(memory_space=pltpu.VMEM), pl.BlockSpec(memory_space=pltpu.HBM)
     return pl.pallas_call(
         serve_body,
-        in_specs=[vmem] * 4 + [hbm],
+        in_specs=[vmem] * 5 + [hbm],
         out_specs=[hbm, hbm],
         out_shape=[pltpu.HBM(down_out.shape, down_out.dtype), pltpu.HBM((tokens, rows), jnp.bfloat16)],
-        input_output_aliases={4: 0},
+        input_output_aliases={5: 0},
         scratch_shapes=[pltpu.VMEM((tokens, rows), jnp.bfloat16), pltpu.SemaphoreType.DMA((2,))],
         compiler_params=pltpu.CompilerParams(vmem_limit_bytes=4 * 1024 * 1024),
         name="serve",
-    )(*hold_in_vmem(down, late, got_late, mine), pltpu.with_memory_space_constraint(down_out, pltpu.HBM))
+    )(*hold_in_vmem(down, late, scaled, got_late, mine), pltpu.with_memory_space_constraint(down_out, pltpu.HBM))
 
 
 def direct_shards(
@@ -707,7 +718,7 @@
     )
     gate_local, up_local, down_some, token = store(wide, down)
     late, got_late, mine = finish(down, scaled, got, token, groups)
-    down_local, mixed = serve(down, late, got_late, mine, down_some)
+    down_local, mixed = serve(down, late, scaled, got_late, mine, down_some)
     return (gate_local, up_local, down_local, mixed)
 
 

time: 212 us -> 212 us (level)
  no operation moved by 1% of the time
where the time goes in v5:
time: 212 us; the launch traced here: 211 us
  Pallas kernels  211 us (100%)
    pallas_call x1, Pallas kernels, spread(): pl.pallas_call(spread_body, in_specs=[pl.BlockSpec(memory_space=pltpu.HBM...  178 us
    pallas_call x1, Pallas kernels, finish(): pl.pallas_call(finish_body, in_specs=[vmem, vmem, vmem, hbm], out_specs=[...  24.2 us
    pallas_call x1, Pallas kernels, store(): pl.pallas_call(store_body, in_specs=[vmem, vmem], out_specs=[hbm, hbm, hb...  7.04 us

profile of v5, /device:TPU:1, one launch (start us, length us, event | category | flops | bytes accessed | tf_op | source)
XLA Modules:
  0.0 211.5 jit_solution(1460225715057241588)
XLA Ops:
  0.6 177.5 %spread.1 = (bf16[2,4,2048,512]{3,2,1,0:T(8,128)(2,1)S(1)}, bf16[4,2048,512]{2,1,0:T(8,128)(2,1)S(1)}, bf16[4,256,512]{2,1,0:T(8,128)(2,1)S(1)}, bf16[7,256,256]{2,1,0:T(8,128)(2,1)S(1)}) custom-call(f32[1,256]{1,0:T(1,128)} %bitcast.12, f32[8,4,256,128]{3,2,1,0:T(8,128)} %bitcast.7, f32[8,4,256,128]{3,2,1,0:T(8,128)} %bitcast.8, ...), custom_call_target="tpu_custom_call" | custom-call | tf_op jit(solution)/shard_map/spread/pallas_call | solution.py:401
  178.2 7.0 %store.1 = (bf16[2048,2048]{1,0:T(8,128)(2,1)}, bf16[2048,2048]{1,0:T(8,128)(2,1)}, bf16[2048,2048]{1,0:T(8,128)(2,1)}, f32[8,128]{1,0:T(8,128)}) custom-call(bf16[2,4,2048,512]{3,2,1,0:T(8,128)(2,1)S(1)} %get-tuple-element.17.wide, bf16[4,2048,512]{2,1,0:T(8,128)(2,1)S(1)} %get-tuple-element.18.down), custom_call_target="tpu_custom_call" | custom-call | tf_op jit(solution)/shard_map/store/pallas_call | solution.py:504
  185.2 24.2 %finish.1 = (bf16[3,4,256,512]{3,2,1,0:T(8,128)(2,1)S(1)}, bf16[3,256,256]{2,1,0:T(8,128)(2,1)S(1)}, f32[256,256]{1,0:T(8,128)S(1)}) custom-call(bf16[4,2048,512]{2,1,0:T(8,128)(2,1)S(1)} %get-tuple-element.18.down, bf16[4,256,512]{2,1,0:T(8,128)(2,1)S(1)} %get-tuple-element.21.scaled, bf16[7,256,256]{2,1,0:T(8,128)(2,1)S(1)} %get-tuple-element.22.got, ...), custom_call_target="tpu_custom_call" | custom-call | tf_op jit(solution)/shard_map/finish/pallas_call | solution.py:632
  209.4 2.1 serve.1
